TPU v7x, 512 devices: a whole 4x8x8 slice. The times are simulated.
512 devices in a mesh: sp: 32 (over z, x), tp: 16 (over y, core).
Axes of the slice: x: 4, y: 8, z: 8, core: 2. Of those that a mesh axis runs over, the one named last changes fastest.
Arguments:
- queries: bfloat16 [8192, 1024], P('sp', 'tp'), may hold values from -6 to 6
- keys: bfloat16 [8192, 256], P('sp'), may hold values from -6 to 6
- values: bfloat16 [8192, 256], P('sp'), may hold values from -6 to 6
- sink: float32 [16], P('tp'), may hold values from 3 to 6
- w_out: bfloat16 [1024, 2048], P('tp'), may hold values from -0.1875 to 0.1875
- stream: bfloat16 [8192, 2048], P(('sp', 'tp')), may hold values from -6 to 6
- gain: bfloat16 [2048], replicated, may hold values from 0.099609375 to 1.8984375
- routes: int32 [8192, 4], P('sp'), may hold values from 0 to 63, all different within a row; in each aligned block of 16 rows (0 to 15, 16 to 31, ...) at most 2 rows name the same one
- route_weights: float32 [8192, 4], P('sp'), may hold values from 0.2 to 1
- w_gate: bfloat16 [64, 1024, 2048], P('sp', 'tp'), may hold values from -0.125 to 0.125
- w_up: bfloat16 [64, 1024, 2048], P('sp', 'tp'), may hold values from -0.125 to 0.125
- w_down: bfloat16 [64, 1024, 2048], P('sp', None, 'tp'), may hold values from -0.1875 to 0.1875
- shared_gate: bfloat16 [1024, 2048], P('tp'), may hold values from -0.125 to 0.125
- shared_up: bfloat16 [1024, 2048], P('tp'), may hold values from -0.125 to 0.125
- shared_down: bfloat16 [1024, 2048], P(None, 'tp'), may hold values from -0.1875 to 0.1875
Outputs:
- layer_out: bfloat16 [8192, 2048], P('sp', 'tp')
Inputs may be any that keep to these rules, and one draw needn't show every extreme that they name: `routes`: in each aligned block of 16 rows no expert is named in more than 2 rows, and some blocks reach 2; a row names 4 different experts.
All inputs are finite; a program needn't handle non-finite values.
Results may differ from a plain program's by a relative error of at most 0.014.
Values may be sent and summed in bfloat16 or wider, within the bound.
A program may use at most 64 MiB of HBM per device.

v0:
```python
import jax
import jax.numpy as jnp
from jax import lax
from jax.sharding import PartitionSpec as P

D = 2048
HEADS = 16
KV_HEADS = 4
HD = 64
WINDOW = 128
EXPERTS = 64
TOPK = 4
NORM_EPS = 1e-05


def with_halo(array, sides, width):
    for axis, dim in sides:
        devices, length = (lax.axis_size(axis), array.shape[dim])
        up = [(i, (i + 1) % devices) for i in range(devices - 1)]
        down = [(j, i) for i, j in up]
        last = lax.slice_in_dim(array, length - width, length, axis=dim)
        leading = lax.slice_in_dim(array, 0, width, axis=dim)
        before = lax.ppermute(last, axis, up)
        after = lax.ppermute(leading, axis, down)
        array = jnp.concatenate([before, array, after], axis=dim)
    return array


def laid_out(tiles, dim):
    tiles = jnp.moveaxis(tiles, 0, dim)
    dims = tiles.shape
    return tiles.reshape(*dims[:dim], dims[dim] * dims[dim + 1], *dims[dim + 2 :])


def from_everyone(array, axis):
    copies = jnp.broadcast_to(array, (lax.axis_size(axis), *array.shape))
    return lax.all_to_all(copies, axis, split_axis=0, concat_axis=0, tiled=True)


def gathered_copies(array, axis, dim):
    return laid_out(from_everyone(array, axis), dim)


def taken_together(array, axis):
    return from_everyone(array, axis).sum(axis=0)


def gather_turned(arrays, axis, dims):
    turned = [jnp.moveaxis(a, dim, 0) for a, dim in zip(arrays, dims)]
    widths = [t[0].size for t in turned]
    both = jnp.concatenate([t.reshape(-1, w) for t, w in zip(turned, widths)], axis=1)
    result = lax.all_gather(both, axis, axis=0, tiled=True)
    tiles = jnp.split(result, [sum(widths[:k]) for k in range(1, len(widths))], axis=1)
    return tuple(
        (
            jnp.moveaxis(b.reshape(-1, *t.shape[1:]), 0, dim)
            for b, t, dim in zip(tiles, turned, dims)
        )
    )


def slot_ids(block_routes, capacity):
    flat_routes = block_routes.reshape(-1)
    hit_table = (flat_routes[:, None] == jnp.arange(EXPERTS)[None, :]).astype(jnp.int32)
    earlier = jnp.cumsum(hit_table, axis=0) - hit_table
    slot_rank = jnp.sum(earlier * hit_table, axis=1)
    return flat_routes * capacity + slot_rank


def local(
    queries,
    keys,
    values,
    sink,
    w_out,
    stream,
    gain,
    routes,
    route_weights,
    w_gate,
    w_up,
    w_down,
    shared_gate,
    shared_up,
    shared_down,
):
    tok_dev = queries.shape[0]
    n_tp = lax.axis_size("tp")
    n_sp = lax.axis_size("sp")
    tp_idx = lax.axis_index("tp")
    sp_idx = lax.axis_index("sp")
    heads_dev = HEADS // n_tp
    group = HEADS // KV_HEADS
    kv_head = tp_idx * heads_dev // group
    key_own = lax.dynamic_slice_in_dim(keys, kv_head * HD, HD, 1)
    value_own = lax.dynamic_slice_in_dim(values, kv_head * HD, HD, 1)
    paired = jnp.concatenate([key_own, value_own], axis=1)
    padded = with_halo(paired, (("sp", 0),), WINDOW)
    blocks = tok_dev // WINDOW
    framed = padded.reshape(blocks + 2, WINDOW, 2 * HD)
    banded = jnp.concatenate([framed[:-2], framed[1:-1], framed[2:]], axis=1)
    key_band = banded[:, :, :HD]
    value_band = banded[:, :, HD:]
    query_blocks = queries.reshape(blocks, WINDOW, heads_dev, HD)
    scores = jnp.einsum(
        "nqhd,njd->nhqj", query_blocks, key_band, preferred_element_type=jnp.float32
    ) * HD ** (-0.5)
    offset = sp_idx * tok_dev
    seq_total = tok_dev * n_sp
    query_pos = (
        offset + jnp.arange(blocks)[:, None, None] * WINDOW + jnp.arange(WINDOW)[None, :, None]
    )
    key_pos = (
        offset
        - WINDOW
        + jnp.arange(blocks)[:, None, None] * WINDOW
        + jnp.arange(3 * WINDOW)[None, None, :]
    )
    allowed = (jnp.abs(query_pos - key_pos) <= WINDOW) & (key_pos >= 0) & (key_pos < seq_total)
    scores = jnp.where(allowed[:, None], scores, -jnp.inf)
    sink_level = sink.reshape(1, heads_dev, 1, 1)
    row_peak = jnp.maximum(scores.max(-1, keepdims=True), sink_level)
    probabilities = jnp.exp(scores - row_peak)
    denominator = probabilities.sum(-1, keepdims=True) + jnp.exp(sink_level - row_peak)
    weights = (probabilities / denominator).astype(jnp.bfloat16)
    attended = jnp.einsum("nhqj,njd->nqhd", weights, value_band, preferred_element_type=jnp.float32)
    attended = attended.astype(jnp.bfloat16).reshape(tok_dev, heads_dev * HD)
    rows_dev = tok_dev // n_tp
    d_dev = w_down.shape[2]
    all_heads = gathered_copies(attended, "tp", 1)
    w_cols, stream_cols = (
        lax.all_to_all(w_out, "tp", split_axis=1, concat_axis=0, tiled=True),
        lax.all_to_all(stream, "tp", split_axis=1, concat_axis=0, tiled=True),
    )
    projected = jnp.dot(all_heads, w_cols, preferred_element_type=jnp.float32)
    mixed_cols = (stream_cols.astype(jnp.float32) + projected).astype(jnp.bfloat16)
    residual = mixed_cols.astype(jnp.float32)
    square_sum = taken_together(jnp.sum(residual * residual, axis=-1), "tp")
    scale_rows = lax.rsqrt(square_sum[:, None] / D + NORM_EPS)
    gain_cols = lax.dynamic_slice_in_dim(gain, tp_idx * d_dev, d_dev, 0).astype(jnp.float32)
    normed_cols = (residual * scale_rows * gain_cols[None, :]).astype(jnp.bfloat16)
    normed = gathered_copies(normed_cols, "tp", 1)
    exp_dev = w_gate.shape[0]
    capacity = max(1, 2 * tok_dev * TOPK // (n_tp * EXPERTS))
    slot_count = EXPERTS * capacity
    blocked_routes = routes.reshape(n_tp, rows_dev, TOPK)
    destination = jax.vmap(lambda block_routes: slot_ids(block_routes, capacity))(blocked_routes)
    slot_select = destination[:, None, :] == jnp.arange(slot_count)[None, :, None]
    slot_select = slot_select.reshape(n_tp, slot_count, rows_dev, TOPK).astype(jnp.float32)
    dispatch_table = jnp.sum(slot_select, axis=-1).astype(jnp.bfloat16)
    combine_table = jnp.sum(slot_select * route_weights.reshape(n_tp, 1, rows_dev, TOPK), axis=-1)
    normed_blocks = normed.reshape(n_tp, rows_dev, D)
    own_table = lax.dynamic_index_in_dim(dispatch_table, tp_idx, 0, keepdims=False)
    own_rows = lax.dynamic_index_in_dim(normed_blocks, tp_idx, 0, keepdims=False)
    outgoing = jnp.dot(own_table, own_rows, preferred_element_type=jnp.float32).astype(jnp.bfloat16)
    arrived = lax.all_to_all(outgoing, "sp", split_axis=0, concat_axis=0, tiled=True)
    arrived = arrived.reshape(1, n_sp, exp_dev, capacity, D)
    piece_rows = lax.all_gather(arrived, "tp", axis=0, tiled=True)
    gate_act = jnp.einsum(
        "tsecd,efd->tsecf", piece_rows, w_gate, preferred_element_type=jnp.float32
    )
    up_act = jnp.einsum("tsecd,efd->tsecf", piece_rows, w_up, preferred_element_type=jnp.float32)
    hidden = (jax.nn.silu(gate_act) * up_act).astype(jnp.bfloat16)
    shared_gate_act = jnp.einsum(
        "td,fd->tf", normed, shared_gate, preferred_element_type=jnp.float32
    )
    shared_up_act = jnp.einsum("td,fd->tf", normed, shared_up, preferred_element_type=jnp.float32)
    shared_hidden = (jax.nn.silu(shared_gate_act) * shared_up_act).astype(jnp.bfloat16)
    shared_hidden = shared_hidden.reshape(1, 1, 1, tok_dev, shared_hidden.shape[1])
    expert_piece, shared_piece = gather_turned((hidden, shared_hidden), "tp", (4, 4))
    piece_width = expert_piece.shape[4]
    routed_total = jnp.einsum(
        "tsecf,efd->tsecd", expert_piece, w_down, preferred_element_type=jnp.float32
    )
    shared_total = jnp.dot(
        shared_piece.reshape(tok_dev, piece_width), shared_down, preferred_element_type=jnp.float32
    )
    returned = lax.all_to_all(
        routed_total.astype(jnp.bfloat16), "sp", split_axis=1, concat_axis=1, tiled=True
    )
    returned = returned.reshape(n_tp, slot_count, d_dev).astype(jnp.float32)
    routed = jnp.einsum("tmr,tmd->trd", combine_table, returned)
    routed = routed.reshape(tok_dev, d_dev)
    return (residual + routed + shared_total).astype(jnp.bfloat16)


def solution(mesh):
    placed = (
        P("sp", "tp"),
        P("sp", None),
        P("sp", None),
        P("tp"),
        P("tp", None),
        P(("sp", "tp"), None),
        P(),
        P("sp", None),
        P("sp", None),
        P("sp", "tp", None),
        P("sp", "tp", None),
        P("sp", None, "tp"),
        P("tp", None),
        P("tp", None),
        P(None, "tp"),
    )
    return jax.shard_map(
        local, mesh=mesh, in_specs=placed, out_specs=P("sp", "tp"), check_vma=False
    )
```

profile of v0, /device:TPU:8, one launch (start us, length us, event | category | flops | bytes accessed | tf_op | source)
XLA Modules:
  0.0 313.8 jit_solution(5770819059560762188)
XLA Ops:
  6.5 1.5 copy_bitcast_fusion.1
  8.1 9.1 %all-to-all-start = ((bf16[16,16,128]{2,0,1:T(8,128)(2,1)}), bf16[16,16,128]{2,0,1:T(8,128)(2,1)S(1)}, u32[]{:S(2)}, u32[]{:S(2)}) async-start(bf16[16,16,128]{2,0,1:T(8,128)(2,1)} %copy_bitcast_fusion.1), calls=%async_computation | async-start | bytes 131072 | tf_op jit(solution)/shard_map/all_to_all | solution.py:133
  17.2 1.0 constant_dynamic-slice_fusion
  18.1 0.1 fusion.40
  18.2 1.9 collective-permute-start
  20.1 1.3 collective-permute-start.1
  21.6 1.7 copy_bitcast_fusion
  24.1 1.9 collective-permute-done.1
  25.9 0.1 pad_maximum_fusion.4
  26.0 0.1 copy.127
  26.2 0.1 copy.129
  26.3 0.1 copy.128
  26.5 1.3 fusion.51
  27.8 7.2 %all-to-all-start.2 = ((bf16[64,16,128]{2,0,1:T(8,128)(2,1)}), bf16[64,16,128]{2,0,1:T(8,128)(2,1)S(1)}, u32[]{:S(2)}, u32[]{:S(2)}) async-start(bf16[64,16,128]{2,0,1:T(8,128)(2,1)} %copy_bitcast_fusion), calls=%async_computation.2 | async-start | bytes 524288 | tf_op jit(solution)/shard_map/all_to_all | solution.py:132
  35.2 0.2 fusion.19
  35.4 9.2 %all-to-all-done.2 = bf16[64,16,128]{2,0,1:T(8,128)(2,1)S(1)} async-done(((bf16[64,16,128]{2,0,1:T(8,128)(2,1)}), bf16[64,16,128]{2,0,1:T(8,128)(2,1)S(1)}, u32[]{:S(2)}, u32[]{:S(2)}) %all-to-all-start.2) | async-done | bytes 262176 | tf_op jit(solution)/shard_map/all_to_all | solution.py:132
  44.7 0.8 broadcast_in_dim.11
  45.5 5.0 %all-to-all-start.1 = ((bf16[16,256,64]{1,2,0:T(8,128)(2,1)}), bf16[16,256,64]{1,2,0:T(8,128)(2,1)S(1)}, u32[]{:S(2)}, u32[]{:S(2)}) async-start(bf16[16,256,64]{1,2,0:T(8,128)(2,1)} %broadcast_in_dim.11), calls=%async_computation.1 | async-start | bytes 1048576 | tf_op jit(solution)/shard_map/all_to_all | solution.py:37
  50.6 0.1 copy.134
  50.7 14.4 %all-to-all-done.1 = bf16[16,256,64]{1,2,0:T(8,128)(2,1)S(1)} async-done(((bf16[16,256,64]{1,2,0:T(8,128)(2,1)}), bf16[16,256,64]{1,2,0:T(8,128)(2,1)S(1)}, u32[]{:S(2)}, u32[]{:S(2)}) %all-to-all-start.1) | async-done | bytes 524320 | tf_op jit(solution)/shard_map/all_to_all | solution.py:37
  65.1 0.3 multiply_reduce_fusion
  65.4 0.6 broadcast_in_dim.12
  66.0 5.7 %all-to-all-start.3 = ((f32[16,1,256]{2,1,0:T(1,128)}), f32[16,1,256]{2,1,0:T(1,128)S(1)}, u32[]{:S(2)}, u32[]{:S(2)}) async-start(f32[16,1,256]{2,1,0:T(1,128)} %broadcast_in_dim.12), calls=%async_computation.3 | async-start | bytes 32768 | tf_op jit(solution)/shard_map/all_to_all | solution.py:37
  71.7 0.8 dynamic-slice_convert_fusion.1
  72.4 5.5 %all-to-all-done.3 = f32[16,1,256]{2,1,0:T(1,128)S(1)} async-done(((f32[16,1,256]{2,1,0:T(1,128)}), f32[16,1,256]{2,1,0:T(1,128)S(1)}, u32[]{:S(2)}, u32[]{:S(2)}) %all-to-all-start.3) | async-done | bytes 16416 | tf_op jit(solution)/shard_map/all_to_all | solution.py:37
  78.0 0.1 multiply_convert_fusion
  78.1 1.1 broadcast_in_dim.13
  79.2 4.9 %all-to-all-start.4 = ((bf16[16,256,128]{1,2,0:T(8,128)(2,1)}), bf16[16,256,128]{1,2,0:T(8,128)(2,1)S(1)}, u32[]{:S(2)}, u32[]{:S(2)}) async-start(bf16[16,256,128]{1,2,0:T(8,128)(2,1)} %broadcast_in_dim.13), calls=%async_computation.4 | async-start | bytes 2097152 | tf_op jit(solution)/shard_map/all_to_all | solution.py:37
  84.1 0.1 copy.135
  84.3 0.1 mul.106
  84.5 0.1 eq.29
  84.6 0.1 copy.136
  84.7 1.4 select_reduce_fusion.1
  86.1 0.1 copy.137
  86.2 1.0 select_reduce_fusion
  87.2 21.5 %all-to-all-done.4 = bf16[16,256,128]{1,2,0:T(8,128)(2,1)S(1)} async-done(((bf16[16,256,128]{1,2,0:T(8,128)(2,1)}), bf16[16,256,128]{1,2,0:T(8,128)(2,1)S(1)}, u32[]{:S(2)}, u32[]{:S(2)}) %all-to-all-start.4) | async-done | bytes 1048608 | tf_op jit(solution)/shard_map/all_to_all | solution.py:37
  108.7 1.1 copy.141
  109.8 1.3 reshape_reshape.2
  111.1 1.2 convolution_convert_fusion
  112.2 0.2 all_to_all.49
  112.4 33.3 %all_to_all.59 = bf16[32,4,2048]{2,1,0:T(4,128)(2,1)S(1)} all-to-all(bf16[32,4,2048]{2,1,0:T(4,128)(2,1)S(1)} %all_to_all.49), channel_id=1, replica_groups=mesh['sp'=32,'tp'=16] {'sp'}, dimensions={0} | all-to-all | bytes 1048576 | tf_op jit(solution)/shard_map/all_to_all | solution.py:156
  145.7 1.1 copy.142
  146.8 0.2 all-gather.5.cloned.1.call-start
  147.1 0.3 fusion.52
  147.4 1.2 fusion.18
  148.6 0.1 copy.144
  148.8 50.0 %all-gather.3.cloned.1.call-done = bf16[16,32,2,2,2048]{4,1,3,0,2:T(8,128)(2,1)} async-done(((bf16[1,32,2,2,2048]{4,1,3,0,2:T(8,128)(2,1)}), bf16[16,32,2,2,2048]{4,1,3,0,2:T(8,128)(2,1)}) %all-gather.3.cloned.1.call-update) | async-done | bytes 8388624 | tf_op jit(solution)/shard_map/all_gather | solution.py:158
  198.8 5.8 %convolution_bitcast_fusion.1 = f32[64,16,32,2,2]{0,2,4,1,3:T(8,128)S(1)} fusion(bf16[16,32,2,2,2048]{4,1,3,0,2:T(8,128)(2,1)} %all-gather.3.cloned.1.call-done, bf16[2,64,2048]{2,1,0:T(8,128)(2,1)S(1)} %copy-done.2), kind=kOutput, calls=%fused_computation.6 | convolution fusion | flops 536870912 | bytes 9437184 | tf_op jit(solution)/shard_map/tsecd,efd->tsecf/dot_general | solution.py:159
  204.7 2.3 fusion.4
  207.0 0.5 copy.143
  207.5 0.1 pad_maximum_fusion
  207.6 1.0 copy.145
  208.6 44.9 %all-gather.5.cloned.1.call-done = bf16[1024,2304]{1,0:T(8,128)(2,1)} async-done(((bf16[64,2304]{1,0:T(8,128)(2,1)}), bf16[1024,2304]{1,0:T(8,128)(2,1)}) %all-gather.5.cloned.1.call-update) | async-done | bytes 4718608 | tf_op jit(solution)/shard_map/all_gather | solution.py:52
  253.5 4.8 %split.8 = bf16[1024,2048]{1,0:T(8,128)(2,1)} slice(bf16[1024,2304]{1,0:T(8,128)(2,1)} %all-gather.5.cloned.1.call-done), slice={[0:1024], [0:2048]} | slice | bytes 8388608 | tf_op jit(solution)/shard_map/split | solution.py:53
  258.3 6.5 %copy.146 = bf16[1024,2048]{0,1:T(8,128)(2,1)} copy(bf16[1024,2048]{1,0:T(8,128)(2,1)} %split.8) | data formatting | bytes 8388608 | tf_op jit(solution)/shard_map/split | solution.py:53
  264.8 7.2 %reshape.237 = bf16[1024,16,32,2,2]{0,4,3,2,1:T(2,128)(2,1)} reshape(bf16[1024,2048]{0,1:T(8,128)(2,1)} %copy.146) | data formatting | bytes 8388608 | tf_op jit(solution)/shard_map/reshape | solution.py:56
  272.0 3.6 %fusion.8 = bf16[16,32,2,2,128]{4,1,3,0,2:T(8,128)(2,1)S(1)} fusion(bf16[1024,16,32,2,2]{0,4,3,2,1:T(2,128)(2,1)} %reshape.237, bf16[2,1024,128]{2,1,0:T(8,128)(2,1)S(1)} %copy-done), kind=kOutput, calls=%fused_computation.9 | convolution fusion | flops 537133056 | bytes 5242880 | tf_op jit(solution)/shard_map/tsecf,efd->tsecd/dot_general | solution.py:172
  275.6 0.5 copy.148
  276.2 28.2 %all_to_all.60 = bf16[16,32,2,2,128]{4,3,0,2,1:T(2,128)(2,1)S(1)} all-to-all(bf16[16,32,2,2,128]{4,3,0,2,1:T(2,128)(2,1)S(1)} %copy.148), channel_id=1, replica_groups=mesh['sp'=32,'tp'=16] {'sp'}, dimensions={1} | all-to-all | bytes 1048576 | tf_op jit(solution)/shard_map/all_to_all | solution.py:178
  304.4 0.1 copy.149
  304.5 0.3 fusion.28
  304.7 0.1 copy.151
  304.9 1.3 fusion.16
  306.2 0.7 copy.153
  (42 shorter events, 0.7 us)
Async XLA Ops:
  6.5 265.5 %copy-start = (bf16[2,1024,128]{2,1,0:T(8,128)(2,1)S(1)}, bf16[2,1024,128]{2,1,0:T(8,128)(2,1)}, u32[]{:S(2)}) copy-start(bf16[2,1024,128]{2,1,0:T(8,128)(2,1)} %param.26) | copy-start | bytes 1572868
  8.1 19.8 %all-to-all-start = ((bf16[16,16,128]{2,0,1:T(8,128)(2,1)}), bf16[16,16,128]{2,0,1:T(8,128)(2,1)S(1)}, u32[]{:S(2)}, u32[]{:S(2)}) async-start(bf16[16,16,128]{2,0,1:T(8,128)(2,1)} %copy_bitcast_fusion.1), calls=%async_computation | async-start | bytes 131072 | tf_op jit(solution)/shard_map/all_to_all | solution.py:133
  18.2 5.8 %collective-permute-start = (bf16[128,128]{1,0:T(8,128)(2,1)S(1)}, bf16[128,128]{1,0:T(8,128)(2,1)S(1)}, u32[]{:S(2)}, u32[]{:S(2)}) collective-permute-start(bf16[128,128]{1,0:T(8,128)(2,1)S(1)} %get-tuple-element.10), channel_id=1, source_target_pairs={{0,16},{16,32},{32,48},{48,64},{64,80},{80,96},{96,112},{112,128},... | collective-permute-start | bytes 98312 | tf_op jit(solution)/shard_map/ppermute | solution.py:23
  20.1 5.8 %collective-permute-start.1 = (bf16[128,128]{1,0:T(8,128)(2,1)S(1)}, bf16[128,128]{1,0:T(8,128)(2,1)S(1)}, u32[]{:S(2)}, u32[]{:S(2)}) collective-permute-start(bf16[128,128]{1,0:T(8,128)(2,1)S(1)} %get-tuple-element.11), channel_id=1, source_target_pairs={{16,0},{32,16},{48,32},{64,48},{80,64},{96,80},{112,96},{128,112},... | collective-permute-start | bytes 98312 | tf_op jit(solution)/shard_map/ppermute | solution.py:24
  27.8 56.3 %copy-start.6 = (s32[256,4]{0,1:T(4,128)S(1)}, s32[256,4]{0,1:T(4,128)}, u32[]{:S(2)}) copy-start(s32[256,4]{0,1:T(4,128)} %param.22) | copy-start | bytes 12292
  27.8 56.5 %copy-start.7 = (f32[256,4]{0,1:T(4,128)S(1)}, f32[256,4]{0,1:T(4,128)}, u32[]{:S(2)}) copy-start(f32[256,4]{0,1:T(4,128)} %param.23) | copy-start | bytes 12292
  27.8 16.8 %all-to-all-start.2 = ((bf16[64,16,128]{2,0,1:T(8,128)(2,1)}), bf16[64,16,128]{2,0,1:T(8,128)(2,1)S(1)}, u32[]{:S(2)}, u32[]{:S(2)}) async-start(bf16[64,16,128]{2,0,1:T(8,128)(2,1)} %copy_bitcast_fusion), calls=%async_computation.2 | async-start | bytes 524288 | tf_op jit(solution)/shard_map/all_to_all | solution.py:132
  45.5 19.5 %all-to-all-start.1 = ((bf16[16,256,64]{1,2,0:T(8,128)(2,1)}), bf16[16,256,64]{1,2,0:T(8,128)(2,1)S(1)}, u32[]{:S(2)}, u32[]{:S(2)}) async-start(bf16[16,256,64]{1,2,0:T(8,128)(2,1)} %broadcast_in_dim.11), calls=%async_computation.1 | async-start | bytes 1048576 | tf_op jit(solution)/shard_map/all_to_all | solution.py:37
  66.0 12.0 %all-to-all-start.3 = ((f32[16,1,256]{2,1,0:T(1,128)}), f32[16,1,256]{2,1,0:T(1,128)S(1)}, u32[]{:S(2)}, u32[]{:S(2)}) async-start(f32[16,1,256]{2,1,0:T(1,128)} %broadcast_in_dim.12), calls=%async_computation.3 | async-start | bytes 32768 | tf_op jit(solution)/shard_map/all_to_all | solution.py:37
  79.2 29.6 %all-to-all-start.4 = ((bf16[16,256,128]{1,2,0:T(8,128)(2,1)}), bf16[16,256,128]{1,2,0:T(8,128)(2,1)S(1)}, u32[]{:S(2)}, u32[]{:S(2)}) async-start(bf16[16,256,128]{1,2,0:T(8,128)(2,1)} %broadcast_in_dim.13), calls=%async_computation.4 | async-start | bytes 2097152 | tf_op jit(solution)/shard_map/all_to_all | solution.py:37
  84.1 114.7 %all-gather.3.cloned.1.call-start = ((), (), s32[]{:S(2)}) async-start(), calls=%async_computation.7 | async-start | bytes 8912896 | tf_op jit(solution)/shard_map/all_gather | solution.py:158
  84.1 63.0 %copy-start.4 = (bf16[64,2048]{1,0:T(8,128)(2,1)S(1)}, bf16[64,2048]{1,0:T(8,128)(2,1)}, u32[]{:S(2)}) copy-start(bf16[64,2048]{1,0:T(8,128)(2,1)} %param.27) | copy-start | bytes 786436
  109.8 89.0 %copy-start.2 = (bf16[2,64,2048]{2,1,0:T(8,128)(2,1)S(1)}, bf16[2,64,2048]{2,1,0:T(8,128)(2,1)}, u32[]{:S(2)}) copy-start(bf16[2,64,2048]{2,1,0:T(8,128)(2,1)} %param.24) | copy-start | bytes 1572868
  146.8 106.7 %all-gather.5.cloned.1.call-start = ((), (), s32[]{:S(2)}) async-start(), calls=%async_computation.8 | async-start | bytes 5013504 | tf_op jit(solution)/shard_map/all_gather | solution.py:52
  148.8 55.9 %copy-start.8 = (bf16[2,64,2048]{2,1,0:T(8,128)(2,1)S(1)}, bf16[2,64,2048]{2,1,0:T(8,128)(2,1)}, u32[]{:S(2)}) copy-start(bf16[2,64,2048]{2,1,0:T(8,128)(2,1)} %param.25) | copy-start | bytes 1572868
  198.8 5.9 %copy-start.1 = (bf16[16,32,2,2,2048]{4,1,3,0,2:T(8,128)(2,1)S(1)}, bf16[16,32,2,2,2048]{4,1,3,0,2:T(8,128)(2,1)}, u32[]{:S(2)}) copy-start(bf16[16,32,2,2,2048]{4,1,3,0,2:T(8,128)(2,1)} %all-gather.3.cloned.1.call-done) | copy-start | bytes 25165828
  272.0 32.5 %copy-start.5 = (bf16[16,128,16]{1,2,0:T(8,128)(2,1)S(1)}, bf16[16,128,16]{1,2,0:T(8,128)(2,1)}, u32[]{:S(2)}) copy-start(bf16[16,128,16]{1,2,0:T(8,128)(2,1)} %get-tuple-element.5) | copy-start | bytes 196612
  272.0 32.8 %copy-start.3 = (bf16[1024,128]{1,0:T(8,128)(2,1)S(1)}, bf16[1024,128]{1,0:T(8,128)(2,1)}, u32[]{:S(2)}) copy-start(bf16[1024,128]{1,0:T(8,128)(2,1)} %param.29) | copy-start | bytes 786436
Sparse Core Ops, SparseCore 0:
  147.0 51.7 all-gather.2
  208.7 44.7 all-gather.4
where the time goes:
time: 315 us; the launch traced here: 314 us
  waiting for transfers between devices  147 us (47%)
  blocking collectives  61.5 us (20%)
  starting transfers between devices  35.4 us (11%)
  local copies, waits for them, and re-layouts  33.1 us (11%)
  matrix products  17.8 us (6%)
  between operations  14.5 us (5%)
  other arithmetic  4.01 us (1%)
    all_gather x1, waiting for transfers between devices, local(): piece_rows = lax.all_gather(arrived, 'tp', axis=0, tiled=True)  50 us
    all_gather x1, waiting for transfers between devices, gather_turned(): result = lax.all_gather(both, axis, axis=0, tiled=True)  44.9 us
    all_to_all x3, waiting for transfers between devices, from_everyone(): return lax.all_to_all(copies, axis, split_axis=0, concat_axis=0, tiled=True)  41.4 us
    all_to_all x1, blocking collectives, local(): lax.all_to_all(outgoing, 'sp', split_axis=0, concat_axis=0, tiled=True)  33.3 us
    all_to_all x1, blocking collectives, local(): lax.all_to_all(routed_total.astype(jnp.bfloat16), 'sp', split_axis=1, con...  28.2 us
    all_to_all x3, starting transfers between devices, from_everyone(): return lax.all_to_all(copies, axis, split_axis=0, concat_axis=0, tiled=True)  15.6 us
    split x2, local copies, waits for them, and re-layouts, gather_turned(): jnp.split(result, [sum(widths[:k]) for k in range(1, len(widths))], axis=1)  11.3 us
    all_to_all x1, waiting for transfers between devices, local(): lax.all_to_all(w_out, 'tp', split_axis=1, concat_axis=0, tiled=True)  9.24 us
  transfers between devices with their start and end apart: 9, of which 7 were waited for; matrix products, arithmetic and copies ran while one was open for 3% of the time, Pallas kernels for 0%

commit v1 on v0

--- a/solution.py
+++ b/solution.py
@@ -155,7 +155,10 @@
     outgoing = jnp.dot(own_table, own_rows, preferred_element_type=jnp.float32).astype(jnp.bfloat16)
     arrived = lax.all_to_all(outgoing, "sp", split_axis=0, concat_axis=0, tiled=True)
     arrived = arrived.reshape(1, n_sp, exp_dev, capacity, D)
-    piece_rows = lax.all_gather(arrived, "tp", axis=0, tiled=True)
+    size = lax.axis_size("tp")
+    pieces = jnp.stack([arrived for _ in range(size)])
+    pieces = lax.all_to_all(pieces, "tp", split_axis=0, concat_axis=0)
+    piece_rows = jnp.concatenate(pieces, axis=0)
     gate_act = jnp.einsum(
         "tsecd,efd->tsecf", piece_rows, w_gate, preferred_element_type=jnp.float32
     )

time: 315 us -> 454 us (1.44)
  waiting for transfers between devices: 147 us -> 275 us
  starting transfers between devices: 35.4 us -> 42.1 us
    all_to_all x0 -> x1, waiting for transfers between devices: none -> 181 us  [local(): pieces = lax.all_to_all(pieces, 'tp', split_axis=0, concat_axis=0)]
    all_gather x1 -> x0, waiting for transfers between devices: 50 us -> none  [local(): piece_rows = lax.all_gather(arrived, 'tp', axis=0, tiled=True)]
    all_to_all x0 -> x1, starting transfers between devices: none -> 6.74 us  [local(): pieces = lax.all_to_all(pieces, 'tp', split_axis=0, concat_axis=0)]
    all_gather x1, waiting for transfers between devices: 44.9 us -> 40 us  [gather_turned(): result = lax.all_gather(both, axis, axis=0, tiled=True)]
    another operation x0 -> x2, local copies, waits for them, and re-layouts: none -> 4.6 us  [local(): pieces = jnp.stack([arrived for _ in range(size)])]
  transfers between devices with their start and end apart: 9 -> 9, of which waited for: 7 -> 7; matrix products, arithmetic and copies ran while one was open for 3% -> 2% of each run, Pallas kernels for 0% -> 0%
where the time goes in v1:
time: 454 us; the launch traced here: 453 us
  waiting for transfers between devices  275 us (61%)
  blocking collectives  61.5 us (14%)
  starting transfers between devices  42.1 us (9%)
  local copies, waits for them, and re-layouts  36.6 us (8%)
  matrix products  20.1 us (4%)
  between operations  14.4 us (3%)
    all_to_all x1, waiting for transfers between devices, local(): pieces = lax.all_to_all(pieces, 'tp', split_axis=0, concat_axis=0)  181 us
    all_to_all x3, waiting for transfers between devices, from_everyone(): return lax.all_to_all(copies, axis, split_axis=0, concat_axis=0, tiled=True)  42.1 us
    all_gather x1, waiting for transfers between devices, gather_turned(): result = lax.all_gather(both, axis, axis=0, tiled=True)  40 us
    all_to_all x1, blocking collectives, local(): lax.all_to_all(outgoing, 'sp', split_axis=0, concat_axis=0, tiled=True)  33.2 us
    all_to_all x1, blocking collectives, local(): lax.all_to_all(routed_total.astype(jnp.bfloat16), 'sp', split_axis=1, con...  28.2 us
    all_to_all x3, starting transfers between devices, from_everyone(): return lax.all_to_all(copies, axis, split_axis=0, concat_axis=0, tiled=True)  15.6 us
    split x2, local copies, waits for them, and re-layouts, gather_turned(): jnp.split(result, [sum(widths[:k]) for k in range(1, len(widths))], axis=1)  11.3 us
    all_to_all x1, waiting for transfers between devices, local(): lax.all_to_all(w_out, 'tp', split_axis=1, concat_axis=0, tiled=True)  9.24 us
  transfers between devices with their start and end apart: 9, of which 7 were waited for; matrix products, arithmetic and copies ran while one was open for 2% of the time, Pallas kernels for 0%

profile of v1, /device:TPU:8, one launch (start us, length us, event | category | flops | bytes accessed | tf_op | source)
XLA Modules:
  0.0 452.5 jit_solution(2030757616792752890)
XLA Ops:
  6.5 1.5 copy_bitcast_fusion.1
  8.1 9.1 %all-to-all-start = ((bf16[16,16,128]{2,0,1:T(8,128)(2,1)}), bf16[16,16,128]{2,0,1:T(8,128)(2,1)S(1)}, u32[]{:S(2)}, u32[]{:S(2)}) async-start(bf16[16,16,128]{2,0,1:T(8,128)(2,1)} %copy_bitcast_fusion.1), calls=%async_computation | async-start | bytes 131072 | tf_op jit(solution)/shard_map/all_to_all | solution.py:133
  17.2 1.0 constant_dynamic-slice_fusion
  18.1 0.1 fusion.56
  18.2 1.9 collective-permute-start
  20.1 1.3 collective-permute-start.1
  21.6 1.7 copy_bitcast_fusion
  24.0 1.9 collective-permute-done.1
  25.9 0.1 pad_maximum_fusion.4
  26.0 0.1 copy.129
  26.2 0.1 copy.131
  26.3 0.1 copy.130
  26.5 1.3 fusion.67
  27.8 7.2 %all-to-all-start.2 = ((bf16[64,16,128]{2,0,1:T(8,128)(2,1)}), bf16[64,16,128]{2,0,1:T(8,128)(2,1)S(1)}, u32[]{:S(2)}, u32[]{:S(2)}) async-start(bf16[64,16,128]{2,0,1:T(8,128)(2,1)} %copy_bitcast_fusion), calls=%async_computation.2 | async-start | bytes 524288 | tf_op jit(solution)/shard_map/all_to_all | solution.py:132
  35.2 0.2 fusion.35
  35.4 9.2 %all-to-all-done.2 = bf16[64,16,128]{2,0,1:T(8,128)(2,1)S(1)} async-done(((bf16[64,16,128]{2,0,1:T(8,128)(2,1)}), bf16[64,16,128]{2,0,1:T(8,128)(2,1)S(1)}, u32[]{:S(2)}, u32[]{:S(2)}) %all-to-all-start.2) | async-done | bytes 262176 | tf_op jit(solution)/shard_map/all_to_all | solution.py:132
  44.7 0.9 broadcast_in_dim.11
  45.5 5.0 %all-to-all-start.1 = ((bf16[16,256,64]{1,2,0:T(8,128)(2,1)}), bf16[16,256,64]{1,2,0:T(8,128)(2,1)S(1)}, u32[]{:S(2)}, u32[]{:S(2)}) async-start(bf16[16,256,64]{1,2,0:T(8,128)(2,1)} %broadcast_in_dim.11), calls=%async_computation.1 | async-start | bytes 1048576 | tf_op jit(solution)/shard_map/all_to_all | solution.py:37
  50.6 0.1 copy.136
  50.7 14.4 %all-to-all-done.1 = bf16[16,256,64]{1,2,0:T(8,128)(2,1)S(1)} async-done(((bf16[16,256,64]{1,2,0:T(8,128)(2,1)}), bf16[16,256,64]{1,2,0:T(8,128)(2,1)S(1)}, u32[]{:S(2)}, u32[]{:S(2)}) %all-to-all-start.1) | async-done | bytes 524320 | tf_op jit(solution)/shard_map/all_to_all | solution.py:37
  65.1 0.3 multiply_reduce_fusion
  65.4 0.6 broadcast_in_dim.12
  66.0 5.7 %all-to-all-start.3 = ((f32[16,1,256]{2,1,0:T(1,128)}), f32[16,1,256]{2,1,0:T(1,128)S(1)}, u32[]{:S(2)}, u32[]{:S(2)}) async-start(f32[16,1,256]{2,1,0:T(1,128)} %broadcast_in_dim.12), calls=%async_computation.3 | async-start | bytes 32768 | tf_op jit(solution)/shard_map/all_to_all | solution.py:37
  71.7 0.8 dynamic-slice_convert_fusion.1
  72.4 5.5 %all-to-all-done.3 = f32[16,1,256]{2,1,0:T(1,128)S(1)} async-done(((f32[16,1,256]{2,1,0:T(1,128)}), f32[16,1,256]{2,1,0:T(1,128)S(1)}, u32[]{:S(2)}, u32[]{:S(2)}) %all-to-all-start.3) | async-done | bytes 16416 | tf_op jit(solution)/shard_map/all_to_all | solution.py:37
  78.0 0.1 multiply_convert_fusion
  78.1 1.1 broadcast_in_dim.13
  79.2 4.9 %all-to-all-start.4 = ((bf16[16,256,128]{1,2,0:T(8,128)(2,1)}), bf16[16,256,128]{1,2,0:T(8,128)(2,1)S(1)}, u32[]{:S(2)}, u32[]{:S(2)}) async-start(bf16[16,256,128]{1,2,0:T(8,128)(2,1)} %broadcast_in_dim.13), calls=%async_computation.4 | async-start | bytes 2097152 | tf_op jit(solution)/shard_map/all_to_all | solution.py:37
  84.1 0.1 copy.137
  84.4 0.1 eq.29
  84.5 0.1 copy.138
  84.6 1.4 select_reduce_fusion.1
  86.2 0.3 select_reduce_fusion
  86.5 22.2 %all-to-all-done.4 = bf16[16,256,128]{1,2,0:T(8,128)(2,1)S(1)} async-done(((bf16[16,256,128]{1,2,0:T(8,128)(2,1)}), bf16[16,256,128]{1,2,0:T(8,128)(2,1)S(1)}, u32[]{:S(2)}, u32[]{:S(2)}) %all-to-all-start.4) | async-done | bytes 1048608 | tf_op jit(solution)/shard_map/all_to_all | solution.py:37
  108.7 1.1 copy.143
  109.8 1.3 reshape_reshape.2
  111.1 1.2 convolution_convert_fusion
  112.2 0.2 all_to_all.52
  112.4 33.2 %all_to_all.64 = bf16[32,4,2048]{2,1,0:T(4,128)(2,1)S(1)} all-to-all(bf16[32,4,2048]{2,1,0:T(4,128)(2,1)S(1)} %all_to_all.52), channel_id=1, replica_groups=mesh['sp'=32,'tp'=16] {'sp'}, dimensions={0} | all-to-all | bytes 1048576 | tf_op jit(solution)/shard_map/all_to_all | solution.py:156
  145.7 0.3 copy.162
  146.0 4.3 stack.3
  150.3 6.7 %all-to-all-start.6 = ((bf16[16,1,32,2,2,2048]{5,2,4,3,1,0:T(8,128)(2,1)}), bf16[16,1,32,2,2,2048]{5,2,4,3,1,0:T(8,128)(2,1)}, u32[]{:S(2)}, u32[]{:S(2)}) async-start(bf16[16,1,32,2,2,2048]{5,2,4,3,1,0:T(8,128)(2,1)} %stack.3), calls=%async_computation.6 | async-start | bytes 16777216 | tf_op jit(solution)/shard_map/all_to_all | solution.py:160
  157.0 0.2 all-gather.2.cloned.1.call-start
  157.3 0.3 fusion.68
  157.6 0.3 fusion.34
  157.9 0.1 copy.147
  158.0 181.3 %all-to-all-done.6 = bf16[16,1,32,2,2,2048]{5,2,4,3,1,0:T(8,128)(2,1)} async-done(((bf16[16,1,32,2,2,2048]{5,2,4,3,1,0:T(8,128)(2,1)}), bf16[16,1,32,2,2,2048]{5,2,4,3,1,0:T(8,128)(2,1)}, u32[]{:S(2)}, u32[]{:S(2)}) %all-to-all-start.6) | async-done | bytes 8388640 | tf_op jit(solution)/shard_map/all_to_all | solution.py:160
  339.3 5.7 %fusion.9 = f32[64,16,32,2,2]{0,2,4,1,3:T(8,128)S(1)} fusion(bf16[16,1,32,2,2,2048]{5,2,4,3,1,0:T(8,128)(2,1)} %all-to-all-done.6, bf16[2,64,2048]{2,1,0:T(8,128)(2,1)S(1)} %copy-done.6), kind=kOutput, calls=%fused_computation.10 | convolution fusion | flops 536870912 | bytes 9437184 | tf_op jit(solution)/shard_map/tsecd,efd->tsecf/dot_general | solution.py:162
  345.0 5.7 %fusion.18 = bf16[64,16,32,2,2]{0,2,4,1,3:T(8,128)(2,1)S(1)} fusion(bf16[16,1,32,2,2,2048]{5,2,4,3,1,0:T(8,128)(2,1)} %all-to-all-done.6, f32[64,16,32,2,2]{0,2,4,1,3:T(8,128)S(1)} %fusion.9, bf16[2,64,2048]{2,1,0:T(8,128)(2,1)S(1)} %copy-done.7), kind=kOutput, calls=%fused_computation.13 | convolution fusion | flops 537657344 | bytes 9699328 | tf_op jit(solution)/shard_map/tsecd,efd->tsecf/dot_general | solution.py:165
  350.7 0.5 copy.146
  351.2 0.1 pad_maximum_fusion
  351.3 1.0 copy.148
  352.3 40.0 %all-gather.2.cloned.1.call-done = bf16[1024,2304]{1,0:T(8,128)(2,1)} async-done(((bf16[64,2304]{1,0:T(8,128)(2,1)}), bf16[1024,2304]{1,0:T(8,128)(2,1)}) %all-gather.2.cloned.1.call-update) | async-done | bytes 4718608 | tf_op jit(solution)/shard_map/all_gather | solution.py:52
  392.3 4.8 %split.8 = bf16[1024,2048]{1,0:T(8,128)(2,1)} slice(bf16[1024,2304]{1,0:T(8,128)(2,1)} %all-gather.2.cloned.1.call-done), slice={[0:1024], [0:2048]} | slice | bytes 8388608 | tf_op jit(solution)/shard_map/split | solution.py:53
  397.1 6.5 %copy.149 = bf16[1024,2048]{0,1:T(8,128)(2,1)} copy(bf16[1024,2048]{1,0:T(8,128)(2,1)} %split.8) | data formatting | bytes 8388608 | tf_op jit(solution)/shard_map/split | solution.py:53
  403.6 7.2 %reshape.241 = bf16[1024,16,32,2,2]{0,4,3,2,1:T(2,128)(2,1)} reshape(bf16[1024,2048]{0,1:T(8,128)(2,1)} %copy.149) | data formatting | bytes 8388608 | tf_op jit(solution)/shard_map/reshape | solution.py:56
  410.8 3.6 fusion.24
  414.4 0.5 copy.151
  414.9 28.2 %all_to_all.65 = bf16[16,32,2,2,128]{4,3,0,2,1:T(2,128)(2,1)S(1)} all-to-all(bf16[16,32,2,2,128]{4,3,0,2,1:T(2,128)(2,1)S(1)} %copy.151), channel_id=1, replica_groups=mesh['sp'=32,'tp'=16] {'sp'}, dimensions={1} | all-to-all | bytes 1048576 | tf_op jit(solution)/shard_map/all_to_all | solution.py:181
  443.1 0.1 copy.152
  443.3 0.3 fusion.44
  443.5 0.1 copy.154
  443.6 1.3 fusion.32
  445.0 0.7 copy.156
  (40 shorter events, 0.8 us)
Async XLA Ops:
  6.5 404.3 %copy-start = (bf16[2,1024,128]{2,1,0:T(8,128)(2,1)S(1)}, bf16[2,1024,128]{2,1,0:T(8,128)(2,1)}, u32[]{:S(2)}) copy-start(bf16[2,1024,128]{2,1,0:T(8,128)(2,1)} %param.26) | copy-start | bytes 1572868
  8.1 19.8 %all-to-all-start = ((bf16[16,16,128]{2,0,1:T(8,128)(2,1)}), bf16[16,16,128]{2,0,1:T(8,128)(2,1)S(1)}, u32[]{:S(2)}, u32[]{:S(2)}) async-start(bf16[16,16,128]{2,0,1:T(8,128)(2,1)} %copy_bitcast_fusion.1), calls=%async_computation | async-start | bytes 131072 | tf_op jit(solution)/shard_map/all_to_all | solution.py:133
  18.2 5.8 %collective-permute-start = (bf16[128,128]{1,0:T(8,128)(2,1)S(1)}, bf16[128,128]{1,0:T(8,128)(2,1)S(1)}, u32[]{:S(2)}, u32[]{:S(2)}) collective-permute-start(bf16[128,128]{1,0:T(8,128)(2,1)S(1)} %get-tuple-element.10), channel_id=1, source_target_pairs={{0,16},{16,32},{32,48},{48,64},{64,80},{80,96},{96,112},{112,128},... | collective-permute-start | bytes 98312 | tf_op jit(solution)/shard_map/ppermute | solution.py:23
  20.1 5.8 %collective-permute-start.1 = (bf16[128,128]{1,0:T(8,128)(2,1)S(1)}, bf16[128,128]{1,0:T(8,128)(2,1)S(1)}, u32[]{:S(2)}, u32[]{:S(2)}) collective-permute-start(bf16[128,128]{1,0:T(8,128)(2,1)S(1)} %get-tuple-element.11), channel_id=1, source_target_pairs={{16,0},{32,16},{48,32},{64,48},{80,64},{96,80},{112,96},{128,112},... | collective-permute-start | bytes 98312 | tf_op jit(solution)/shard_map/ppermute | solution.py:24
  27.8 56.3 %copy-start.4 = (s32[256,4]{0,1:T(4,128)S(1)}, s32[256,4]{0,1:T(4,128)}, u32[]{:S(2)}) copy-start(s32[256,4]{0,1:T(4,128)} %param.22) | copy-start | bytes 12292
  27.8 56.5 %copy-start.5 = (f32[256,4]{0,1:T(4,128)S(1)}, f32[256,4]{0,1:T(4,128)}, u32[]{:S(2)}) copy-start(f32[256,4]{0,1:T(4,128)} %param.23) | copy-start | bytes 12292
  27.8 16.8 %all-to-all-start.2 = ((bf16[64,16,128]{2,0,1:T(8,128)(2,1)}), bf16[64,16,128]{2,0,1:T(8,128)(2,1)S(1)}, u32[]{:S(2)}, u32[]{:S(2)}) async-start(bf16[64,16,128]{2,0,1:T(8,128)(2,1)} %copy_bitcast_fusion), calls=%async_computation.2 | async-start | bytes 524288 | tf_op jit(solution)/shard_map/all_to_all | solution.py:132
  45.5 19.5 %all-to-all-start.1 = ((bf16[16,256,64]{1,2,0:T(8,128)(2,1)}), bf16[16,256,64]{1,2,0:T(8,128)(2,1)S(1)}, u32[]{:S(2)}, u32[]{:S(2)}) async-start(bf16[16,256,64]{1,2,0:T(8,128)(2,1)} %broadcast_in_dim.11), calls=%async_computation.1 | async-start | bytes 1048576 | tf_op jit(solution)/shard_map/all_to_all | solution.py:37
  66.0 12.0 %all-to-all-start.3 = ((f32[16,1,256]{2,1,0:T(1,128)}), f32[16,1,256]{2,1,0:T(1,128)S(1)}, u32[]{:S(2)}, u32[]{:S(2)}) async-start(f32[16,1,256]{2,1,0:T(1,128)} %broadcast_in_dim.12), calls=%async_computation.3 | async-start | bytes 32768 | tf_op jit(solution)/shard_map/all_to_all | solution.py:37
  79.2 29.6 %all-to-all-start.4 = ((bf16[16,256,128]{1,2,0:T(8,128)(2,1)}), bf16[16,256,128]{1,2,0:T(8,128)(2,1)S(1)}, u32[]{:S(2)}, u32[]{:S(2)}) async-start(bf16[16,256,128]{1,2,0:T(8,128)(2,1)} %broadcast_in_dim.13), calls=%async_computation.4 | async-start | bytes 2097152 | tf_op jit(solution)/shard_map/all_to_all | solution.py:37
  150.3 7.0 %copy-start.2 = (bf16[64,2048]{1,0:T(8,128)(2,1)S(1)}, bf16[64,2048]{1,0:T(8,128)(2,1)}, u32[]{:S(2)}) copy-start(bf16[64,2048]{1,0:T(8,128)(2,1)} %param.27) | copy-start | bytes 786436
  150.3 7.3 %copy-start.3 = (bf16[64,2048]{1,0:T(8,128)(2,1)S(1)}, bf16[64,2048]{1,0:T(8,128)(2,1)}, u32[]{:S(2)}) copy-start(bf16[64,2048]{1,0:T(8,128)(2,1)} %param.28) | copy-start | bytes 786436
  150.3 189.0 %copy-start.6 = (bf16[2,64,2048]{2,1,0:T(8,128)(2,1)S(1)}, bf16[2,64,2048]{2,1,0:T(8,128)(2,1)}, u32[]{:S(2)}) copy-start(bf16[2,64,2048]{2,1,0:T(8,128)(2,1)} %param.24) | copy-start | bytes 1572868
  150.3 189.0 %all-to-all-start.6 = ((bf16[16,1,32,2,2,2048]{5,2,4,3,1,0:T(8,128)(2,1)}), bf16[16,1,32,2,2,2048]{5,2,4,3,1,0:T(8,128)(2,1)}, u32[]{:S(2)}, u32[]{:S(2)}) async-start(bf16[16,1,32,2,2,2048]{5,2,4,3,1,0:T(8,128)(2,1)} %stack.3), calls=%async_computation.6 | async-start | bytes 16777216 | tf_op jit(solution)/shard_map/all_to_all | solution.py:160
  157.0 235.3 %all-gather.2.cloned.1.call-start = ((), (), s32[]{:S(2)}) async-start(), calls=%async_computation.8 | async-start | bytes 5013504 | tf_op jit(solution)/shard_map/all_gather | solution.py:52
  158.0 187.0 %copy-start.7 = (bf16[2,64,2048]{2,1,0:T(8,128)(2,1)S(1)}, bf16[2,64,2048]{2,1,0:T(8,128)(2,1)}, u32[]{:S(2)}) copy-start(bf16[2,64,2048]{2,1,0:T(8,128)(2,1)} %param.25) | copy-start | bytes 1572868
  410.8 32.8 %copy-start.1 = (bf16[1024,128]{1,0:T(8,128)(2,1)S(1)}, bf16[1024,128]{1,0:T(8,128)(2,1)}, u32[]{:S(2)}) copy-start(bf16[1024,128]{1,0:T(8,128)(2,1)} %param.29) | copy-start | bytes 786436
Sparse Core Ops, SparseCore 0:
  352.4 39.8 all-gather.1
